TPU v7x, 32 devices: a whole 2x2x4 slice. The times are simulated.
32 devices in a mesh: rep: 2 (over x), fs: 8 (over z, y), tp: 2 (over core).
Axes of the slice: x: 2, y: 2, z: 4, core: 2. Of those that a mesh axis runs over, the one named last changes fastest.
Arguments:
- tokens: bfloat16 [5120, 2048], P(('rep', 'fs'), 'tp'), may hold values from -30 to 30
- mixer_gain: float32 [2048], P('tp'), may hold values from 0.1 to 1.9
- outer_weight: float32 [2048, 1024], P('fs', 'tp'), may hold values from -0.125 to 0.125
- inner_weight: float32 [2048, 1024], P('fs', 'tp'), may hold values from -0.125 to 0.125
- value_weight: float32 [2048, 1024], P('fs', 'tp'), may hold values from -0.125 to 0.125
- outer_scale: float32 [1024], P(('tp', 'fs')), may hold values from 0.5 to 2
- inner_scale: float32 [1024], P(('tp', 'fs')), may hold values from 0.5 to 2
- value_scale: float32 [1024], P(('tp', 'fs')), may hold values from 0.5 to 2
- mixer_taps: float32 [3, 1024], P(None, 'tp'), may hold values from -3.5 to 3.5
- mixer_project: float32 [1024, 2048], P('tp', 'fs'), may hold values from -0.1875 to 0.1875
- project_scale: float32 [2048], P('fs'), may hold values from 0.5 to 2
- channel_gain: float32 [2048], P('tp'), may hold values from 0.1 to 1.9
- gate_weight: float32 [2048, 5632], P('fs', 'tp'), may hold values from -0.125 to 0.125
- gate_scale: float32 [5632], P(('tp', 'fs')), may hold values from 0.5 to 2
- up_weight: float32 [2048, 5632], P('fs', 'tp'), may hold values from -0.125 to 0.125
- up_scale: float32 [5632], P(('tp', 'fs')), may hold values from 0.5 to 2
- channel_taps: float32 [3, 5632], P(None, 'tp'), may hold values from -3.5 to 3.5
- channel_bias: float32 [5632], P('tp'), may hold values from -3 to 3
- down_weight: float32 [5632, 2048], P('tp', 'fs'), may hold values from -0.078125 to 0.078125
- down_scale: float32 [2048], P('fs'), may hold values from 0.5 to 2
Outputs:
- result: bfloat16 [5120, 2048], P(('rep', 'fs'), 'tp')
All inputs are finite; a program needn't handle non-finite values.
Results may differ from a plain program's by a relative error of at most 0.015.
Values may be sent and summed in bfloat16 or wider, within the bound.
A program may use at most 128 MiB of HBM per device.

v0:
```python
import jax
import jax.numpy as jnp
from jax import lax
from jax.sharding import PartitionSpec as P

LEN = 320
epsilon = 1e-06


def normalize(token_rows, gain):
    values = token_rows.astype(jnp.float32)
    squares = lax.psum(jnp.sum(values * values, axis=1), "tp")
    features = values.shape[1] * lax.axis_size("tp")
    inverse = lax.rsqrt(squares / features + epsilon)
    local = (values * inverse[:, None] * gain).astype(jnp.bfloat16)
    return lax.all_gather(local, "tp", axis=1, tiled=True)


def causal_taps(values, taps):
    tap_count = taps.shape[0]
    grouped = values.reshape(-1, LEN, values.shape[1])
    padded = jnp.pad(grouped, ((0, 0), (tap_count - 1, 0), (0, 0)))
    running = jnp.zeros_like(grouped)
    for offset in range(tap_count):
        running = running + taps[offset] * padded[:, offset : offset + LEN]
    return running.reshape(values.shape)


def accumulate(whole, pieces):
    return tuple(
        (
            jnp.dot(whole, weight_block, preferred_element_type=jnp.float32)
            for weight_block in pieces
        )
    )


def project_back(hidden, weight, scale):
    product = (
        jnp.dot(
            hidden,
            lax.all_gather(weight, "fs", axis=1, tiled=True),
            preferred_element_type=jnp.float32,
        )
        * scale
    )
    partials = lax.optimization_barrier(product.astype(jnp.bfloat16)).astype(jnp.float32)
    return lax.psum_scatter(
        partials.astype(jnp.bfloat16), "tp", scatter_dimension=1, tiled=True
    ).astype(jnp.float32)


def per_device(
    tokens,
    mixer_gain,
    outer_weight,
    inner_weight,
    value_weight,
    outer_scale,
    inner_scale,
    value_scale,
    mixer_taps,
    mixer_project,
    project_scale,
    channel_gain,
    gate_weight,
    gate_scale,
    up_weight,
    up_scale,
    channel_taps,
    channel_bias,
    down_weight,
    down_scale,
):
    outer_full, inner_full, value_full, gate_full, up_full, project_full, down_full = (
        lax.all_gather(outer_scale, "fs", axis=0, tiled=True),
        lax.all_gather(inner_scale, "fs", axis=0, tiled=True),
        lax.all_gather(value_scale, "fs", axis=0, tiled=True),
        lax.all_gather(gate_scale, "fs", axis=0, tiled=True),
        lax.all_gather(up_scale, "fs", axis=0, tiled=True),
        lax.all_gather(project_scale, "fs", axis=0, tiled=True),
        lax.all_gather(down_scale, "fs", axis=0, tiled=True),
    )
    channel_low = (gate_weight.astype(jnp.bfloat16), up_weight.astype(jnp.bfloat16))
    normed = normalize(tokens, mixer_gain)
    mixer_low = (
        outer_weight.astype(jnp.bfloat16),
        inner_weight.astype(jnp.bfloat16),
        value_weight.astype(jnp.bfloat16),
    )
    outer_part, inner_part, value_part = accumulate(
        normed,
        (
            lax.all_gather(mixer_low[0], "fs", axis=0, tiled=True),
            lax.all_gather(mixer_low[1], "fs", axis=0, tiled=True),
            lax.all_gather(mixer_low[2], "fs", axis=0, tiled=True),
        ),
    )
    outer_part = outer_part * outer_full
    conv_input = inner_part * inner_full * (value_part * value_full)
    mixed = (outer_part * causal_taps(conv_input, mixer_taps)).astype(jnp.bfloat16)
    mixer_sum = project_back(mixed, mixer_project.astype(jnp.bfloat16), project_full)
    middle = (tokens.astype(jnp.float32) + mixer_sum).astype(jnp.bfloat16)
    normed_two = normalize(middle, channel_gain)
    gate_part, up_part = accumulate(
        normed_two,
        (
            lax.all_gather(channel_low[0], "fs", axis=0, tiled=True),
            lax.all_gather(channel_low[1], "fs", axis=0, tiled=True),
        ),
    )
    gate_part = gate_part * gate_full
    up_part = up_part * up_full
    hidden = (jax.nn.silu(causal_taps(gate_part, channel_taps) + channel_bias) * up_part).astype(
        jnp.bfloat16
    )
    channel_sum = project_back(hidden, down_weight.astype(jnp.bfloat16), down_full)
    return (middle.astype(jnp.float32) + channel_sum).astype(jnp.bfloat16)


def solution(mesh):
    placed = (
        P(("rep", "fs"), "tp"),
        P("tp"),
        P("fs", "tp"),
        P("fs", "tp"),
        P("fs", "tp"),
        P(("tp", "fs")),
        P(("tp", "fs")),
        P(("tp", "fs")),
        P(None, "tp"),
        P("tp", "fs"),
        P("fs"),
        P("tp"),
        P("fs", "tp"),
        P(("tp", "fs")),
        P("fs", "tp"),
        P(("tp", "fs")),
        P(None, "tp"),
        P("tp"),
        P("tp", "fs"),
        P("fs"),
    )
    return jax.shard_map(
        per_device, mesh=mesh, in_specs=placed, out_specs=P(("rep", "fs"), "tp"), check_vma=False
    )
```

profile of v0, /device:TPU:0, one launch (start us, length us, event | category | flops | bytes accessed | tf_op | source)
XLA Modules:
  0.0 787.0 jit_solution(13122378445534658382)
XLA Ops:
  6.5 1.4 fusion.4
  7.9 2.8 psum.14
  10.7 2.1 fusion.6
  12.9 0.0 all-gather.12.cloned.1.call-update
  12.9 0.0 copy-start.22
  12.9 0.0 copy-start.19
  12.9 0.0 copy-start.10
  13.0 0.0 all-gather.16.cloned.1.call-start
  13.0 0.7 convert_element_type.70
  13.8 0.0 all-gather.16.cloned.1.call-update
  13.8 0.0 all-gather.18.cloned.1.call-start
  13.9 0.7 convert_element_type.71
  14.6 0.0 all-gather.18.cloned.1.call-update
  14.6 0.0 all-gather.14.cloned.1.call-start
  14.7 0.7 convert_element_type.69
  15.4 0.0 all-gather.14.cloned.1.call-update
  15.5 0.0 all-gather.20.cloned.1.call-start
  15.5 0.7 convert_element_type.73
  16.3 0.0 all-gather.20.cloned.1.call-update
  16.3 0.0 reduce-scatter.3.cloned.1.call-start
  16.4 0.7 dynamic-slice
  18.4 0.2 dynamic-update-slice
  18.6 0.2 dynamic-update-slice.1
  18.9 0.2 dynamic-update-slice.2
  19.1 0.3 dynamic-update-slice.3
  19.4 0.3 dynamic-update-slice.4
  19.6 39.4 %all-reduce.7 = (f32[512]{0:T(512)S(1)}, f32[512]{0:T(512)S(1)}, f32[512]{0:T(512)S(1)}, f32[2816]{0:T(1024)}, f32[2816]{0:T(1024)}) all-reduce(f32[512]{0:T(512)S(1)} %dynamic-update-slice.1, f32[512]{0:T(512)S(1)} %dynamic-update-slice.2, f32[512]{0:T(512)S(1)} %dynamic-update-slice, ...), channel_id=1, replica_groups=mesh['rep'=2,'fs'=8,'tp'=2] {'fs'}, use_global_device_ids=true, to_apply=%add.3 | all-reduce | flops 7168 | bytes 57344
  59.0 16.7 %all-gather = f32[8,1,256]{2,1,0:T(1,128)S(1)} all-gather(f32[1,1,256]{2,1,0:T(1,128)S(1)} %bitcast.52), channel_id=1, replica_groups=mesh['rep'=2,'fs'=8,'tp'=2] {'fs'}, dimensions={0}, use_global_device_ids=true | all-gather | bytes 9216 | tf_op jit(solution)/shard_map/all_gather | solution.py:81
  75.8 0.0 all-gather.12.cloned.1.call-done
  75.8 1.8 all-gather.16.cloned.1.call-done
  77.6 2.9 convolution_multiply_fusion.5
  80.5 46.9 %all-gather.18.cloned.1.call-done = bf16[2048,512]{1,0:T(8,128)(2,1)} async-done(((bf16[256,512]{1,0:T(8,128)(2,1)}), bf16[2048,512]{1,0:T(8,128)(2,1)}) %all-gather.18.cloned.1.call-update) | async-done | bytes 2097168 | tf_op jit(solution)/shard_map/all_gather | solution.py:96
  127.4 2.5 fusion.12
  129.9 47.2 %all-gather.14.cloned.1.call-done = bf16[2048,512]{1,0:T(8,128)(2,1)} async-done(((bf16[256,512]{1,0:T(8,128)(2,1)}), bf16[2048,512]{1,0:T(8,128)(2,1)}) %all-gather.14.cloned.1.call-update) | async-done | bytes 2097168 | tf_op jit(solution)/shard_map/all_gather | solution.py:94
  177.0 50.8 %all-gather.20.cloned.1.call-done = bf16[512,2048]{1,0:T(8,128)(2,1)} async-done(((bf16[512,256]{1,0:T(8,128)(2,1)}), bf16[512,2048]{1,0:T(8,128)(2,1)}) %all-gather.20.cloned.1.call-update) | async-done | bytes 2097168 | tf_op jit(solution)/shard_map/all_gather | solution.py:42
  227.8 5.1 fusion.2
  233.0 0.0 reduce-scatter.3.cloned.1.call-update
  233.0 0.0 all-gather.22.cloned.1.call-start
  233.0 6.9 reduce-scatter.3.cloned.1.call-done
  239.9 1.4 fusion.8
  241.3 2.5 psum.15
  243.8 2.2 fusion.10
  246.0 0.0 all-gather.22.cloned.1.call-update
  246.0 0.0 all-gather.24.cloned.1.call-start
  246.1 1.2 convert_element_type.79
  247.3 0.0 all-gather.24.cloned.1.call-update
  247.3 0.0 all-gather.26.cloned.1.call-start
  247.4 3.2 convert_element_type.80
  250.6 0.0 all-gather.26.cloned.1.call-update
  250.6 0.0 all-gather.28.cloned.1.call-start
  250.7 1.2 convert_element_type.82
  251.9 0.0 all-gather.28.cloned.1.call-update
  251.9 0.0 reduce-scatter.5.cloned.1.call-start
  252.0 21.1 %all-gather.1 = f32[8,1,256]{2,1,0:T(1,128)S(1)} all-gather(f32[1,1,256]{2,1,0:T(1,128)S(1)} %bitcast.53), channel_id=1, replica_groups=mesh['rep'=2,'fs'=8,'tp'=2] {'fs'}, dimensions={0}, use_global_device_ids=true | all-gather | bytes 9216 | tf_op jit(solution)/shard_map/all_gather | solution.py:82
  273.1 1.0 slice_reduce_fusion.2
  274.1 0.0 all-gather.22.cloned.1.call-done
  274.1 149.5 %all-gather.24.cloned.1.call-done = bf16[2048,2816]{1,0:T(8,128)(2,1)} async-done(((bf16[256,2816]{1,0:T(8,128)(2,1)}), bf16[2048,2816]{1,0:T(8,128)(2,1)}) %all-gather.24.cloned.1.call-update) | async-done | bytes 11534352 | tf_op jit(solution)/shard_map/all_gather | solution.py:108
  423.6 10.5 %convolution_multiply_fusion.1 = f32[320,2816]{1,0:T(8,128)} fusion(bf16[320,2048]{1,0:T(8,128)(2,1)} %all-gather.22.cloned.1.call-done, bf16[2048,2816]{1,0:T(8,128)(2,1)} %all-gather.24.cloned.1.call-done, f32[2816]{0:T(1024)S(1)} %copy-done.18), kind=kOutput, calls=%fused_computation.2 | convolution fusion | flops 3691888640 | bytes 16460800 | tf_op jit(solution)/shard_map/dot_general | solution.py:32
  434.1 153.2 %all-gather.26.cloned.1.call-done = bf16[2048,2816]{1,0:T(8,128)(2,1)} async-done(((bf16[256,2816]{1,0:T(8,128)(2,1)}), bf16[2048,2816]{1,0:T(8,128)(2,1)}) %all-gather.26.cloned.1.call-update) | async-done | bytes 11534352 | tf_op jit(solution)/shard_map/all_gather | solution.py:109
  587.3 163.4 %all-gather.28.cloned.1.call-done = bf16[2816,2048]{1,0:T(8,128)(2,1)} async-done(((bf16[2816,256]{1,0:T(8,128)(2,1)}), bf16[2816,2048]{1,0:T(8,128)(2,1)}) %all-gather.28.cloned.1.call-update) | async-done | bytes 11534352 | tf_op jit(solution)/shard_map/all_gather | solution.py:42
  750.7 20.5 %fusion.3 = bf16[320,2048]{1,0:T(8,128)(2,1)} fusion(bf16[2816,2048]{1,0:T(8,128)(2,1)} %all-gather.28.cloned.1.call-done, f32[2048]{0:T(1024)S(1)} %bitcast.48, bf16[320,2048]{1,0:T(8,128)(2,1)S(1)} %copy-done.15, bf16[2048,2816]{1,0:T(8,128)(2,1)} %all-gather.26.cloned.1.call-done, f32[320,2816]{1,0:T(8,128)} %convolution_multiply_fusion.1, ...), kind=kOutput, calls=%fused_computation.9 | convolution fusion | flops 7395000320 | bytes 32963584 | tf_op jit(solution)/shard_map/dot_general | solution.py:40
  771.2 0.0 reduce-scatter.5.cloned.1.call-update
  771.3 6.9 reduce-scatter.5.cloned.1.call-done
  778.2 2.3 fusion.11
  (52 shorter events, 0.1 us)
Async XLA Ops:
  6.5 6.5 copy-start.4
  6.5 7.3 copy-start.5
  6.5 69.2 %all-gather.12.cloned.1.call-start = ((), (), s32[]{:S(2)}) async-start(), calls=%async_computation.2 | async-start | bytes 1966080 | tf_op jit(solution)/shard_map/all_gather | solution.py:16
  7.9 6.7 copy-start.6
  12.9 2.7 copy-start.7
  12.9 3.5 copy-start.22
  12.9 5.5 copy-start.19
  12.9 5.7 copy-start.20
  12.9 5.9 copy-start.21
  12.9 6.2 copy-start.10
  12.9 6.4 copy-start.11
  13.0 46.0 %copy-start.12 = (f32[256]{0:T(256)S(1)}, f32[256]{0:T(256)}, u32[]{:S(2)}) copy-start(f32[256]{0:T(256)} %param.30) | copy-start | bytes 3076
  13.0 62.8 %copy-start.8 = (f32[3,512]{1,0:T(4,128)S(1)}, f32[3,512]{1,0:T(4,128)}, u32[]{:S(2)}) copy-start(f32[3,512]{1,0:T(4,128)} %param.28) | copy-start | bytes 18436
  13.0 64.6 %all-gather.16.cloned.1.call-start = ((), (), s32[]{:S(2)}) async-start(), calls=%async_computation.4 | async-start | bytes 2359296 | tf_op jit(solution)/shard_map/all_gather | solution.py:95
  13.8 113.6 %all-gather.18.cloned.1.call-start = ((), (), s32[]{:S(2)}) async-start(), calls=%async_computation.5 | async-start | bytes 2359296 | tf_op jit(solution)/shard_map/all_gather | solution.py:96
  14.6 162.4 %all-gather.14.cloned.1.call-start = ((), (), s32[]{:S(2)}) async-start(), calls=%async_computation.3 | async-start | bytes 2359296 | tf_op jit(solution)/shard_map/all_gather | solution.py:94
  15.5 212.4 %all-gather.20.cloned.1.call-start = ((), (), s32[]{:S(2)}) async-start(), calls=%async_computation.6 | async-start | bytes 2359296 | tf_op jit(solution)/shard_map/all_gather | solution.py:42
  16.3 223.6 %reduce-scatter.3.cloned.1.call-start = ((), (), s32[]{:S(2)}) async-start(), calls=%async_computation.7 | async-start | bytes 1966080 | tf_op jit(solution)/shard_map/reduce_scatter | solution.py:48
  77.6 49.8 %copy-start.14 = (bf16[320,2048]{1,0:T(8,128)(2,1)S(1)}, bf16[320,2048]{1,0:T(8,128)(2,1)}, u32[]{:S(2)}) copy-start(bf16[320,2048]{1,0:T(8,128)(2,1)} %all-gather.12.cloned.1.call-done) | copy-start | bytes 3932164
  227.8 12.1 %copy-start = (bf16[320,1024]{1,0:T(8,128)(2,1)S(1)}, bf16[320,1024]{1,0:T(8,128)(2,1)}, u32[]{:S(2)}) copy-start(bf16[320,1024]{1,0:T(8,128)(2,1)} %param.20) | copy-start | bytes 1966084
  232.9 10.8 %copy-start.9 = (f32[1024]{0:T(1024)S(1)}, f32[1024]{0:T(1024)}, u32[]{:S(2)}) copy-start(f32[1024]{0:T(1024)} %param.31) | copy-start | bytes 12292
  233.0 13.1 %copy-start.2 = (f32[256,2816]{1,0:T(8,128)S(1)}, f32[256,2816]{1,0:T(8,128)}, u32[]{:S(2)}) copy-start(f32[256,2816]{1,0:T(8,128)} %param.32) | copy-start | bytes 8650756
  233.0 41.1 %all-gather.22.cloned.1.call-start = ((), (), s32[]{:S(2)}) async-start(), calls=%async_computation.8 | async-start | bytes 1966080 | tf_op jit(solution)/shard_map/all_gather | solution.py:16
  246.0 177.6 %all-gather.24.cloned.1.call-start = ((), (), s32[]{:S(2)}) async-start(), calls=%async_computation.9 | async-start | bytes 12976128 | tf_op jit(solution)/shard_map/all_gather | solution.py:108
  247.3 3.4 copy-start.3
  247.3 340.0 %all-gather.26.cloned.1.call-start = ((), (), s32[]{:S(2)}) async-start(), calls=%async_computation.10 | async-start | bytes 12976128 | tf_op jit(solution)/shard_map/all_gather | solution.py:109
  250.6 1.4 copy-start.13
  250.6 173.0 %copy-start.18 = (f32[2816]{0:T(1024)S(1)}, f32[2816]{0:T(1024)}, u32[]{:S(2)}) copy-start(f32[2816]{0:T(1024)} %get-tuple-element.11) | copy-start | bytes 33796
  250.6 500.1 %all-gather.28.cloned.1.call-start = ((), (), s32[]{:S(2)}) async-start(), calls=%async_computation.11 | async-start | bytes 12976128 | tf_op jit(solution)/shard_map/all_gather | solution.py:42
  251.9 526.3 %reduce-scatter.5.cloned.1.call-start = ((), (), s32[]{:S(2)}) async-start(), calls=%async_computation.12 | async-start | bytes 1966080 | tf_op jit(solution)/shard_map/reduce_scatter | solution.py:48
  423.6 327.1 %copy-start.15 = (bf16[320,2048]{1,0:T(8,128)(2,1)S(1)}, bf16[320,2048]{1,0:T(8,128)(2,1)}, u32[]{:S(2)}) copy-start(bf16[320,2048]{1,0:T(8,128)(2,1)} %all-gather.22.cloned.1.call-done) | copy-start | bytes 3932164
  423.6 327.1 %copy-start.16 = (f32[2816]{0:T(1024)S(1)}, f32[2816]{0:T(1024)}, u32[]{:S(2)}) copy-start(f32[2816]{0:T(1024)} %param.37) | copy-start | bytes 33796
  423.6 327.1 %copy-start.17 = (f32[2816]{0:T(1024)S(1)}, f32[2816]{0:T(1024)}, u32[]{:S(2)}) copy-start(f32[2816]{0:T(1024)} %get-tuple-element.12) | copy-start | bytes 33796
  750.7 27.5 %copy-start.1 = (bf16[320,1024]{1,0:T(8,128)(2,1)S(1)}, bf16[320,1024]{1,0:T(8,128)(2,1)}, u32[]{:S(2)}) copy-start(bf16[320,1024]{1,0:T(8,128)(2,1)} %reduce-scatter.3.cloned.1.call-done) | copy-start | bytes 1966084
Sparse Core Ops, SparseCore 0:
  13.0 11.9 all-gather.11
  27.1 50.3 all-gather.15
  79.7 47.6 all-gather.17
  129.4 47.6 all-gather.13
  178.9 48.8 all-gather.19
  233.1 6.7 reduce-scatter.2
  246.1 10.6 all-gather.21
  259.0 164.4 all-gather.23
  425.8 161.4 all-gather.25
  589.2 161.4 all-gather.27
  771.4 6.7 reduce-scatter.4
where the time goes:
time: 787 us
  waiting for transfers between devices  627 us (80%)
  blocking collectives  82.4 us (10%)
  matrix products  41.5 us (5%)
  other arithmetic  18 us (2%)
  between operations  14.8 us (2%)
    all_gather x2, waiting for transfers between devices, project_back(): lax.all_gather(weight, 'fs', axis=1, tiled=True)  214 us
    all_gather x1, waiting for transfers between devices, per_device(): lax.all_gather(channel_low[1], 'fs', axis=0, tiled=True)  153 us
    all_gather x1, waiting for transfers between devices, per_device(): lax.all_gather(channel_low[0], 'fs', axis=0, tiled=True)  149 us
    all_gather x1, waiting for transfers between devices, per_device(): lax.all_gather(mixer_low[0], 'fs', axis=0, tiled=True)  47.2 us
    all_gather x1, waiting for transfers between devices, per_device(): lax.all_gather(mixer_low[2], 'fs', axis=0, tiled=True)  46.9 us
    unnamed x1, blocking collectives  39.4 us
    dot_general x2, matrix products, project_back(): jnp.dot(hidden, lax.all_gather(weight, 'fs', axis=1, tiled=True), preferr...  25.6 us
    all_gather x1, blocking collectives, per_device(): lax.all_gather(down_scale, 'fs', axis=0, tiled=True)  21.1 us
  transfers between devices with their start and end apart: 11, of which 9 were waited for; matrix products, arithmetic and copies ran while one was open for 3% of the time, Pallas kernels for 0%

commit v1 on v0

--- a/solution.py
+++ b/solution.py
@@ -5,6 +5,11 @@
 
 LEN = 320
 epsilon = 1e-06
+
+
+def _serve_tracks(x_local):
+    frame_out = lax.all_gather(x_local, "fs")
+    return jnp.concatenate(frame_out, axis=1)
 
 
 def normalize(token_rows, gain):
@@ -36,14 +41,7 @@
 
 
 def project_back(hidden, weight, scale):
-    product = (
-        jnp.dot(
-            hidden,
-            lax.all_gather(weight, "fs", axis=1, tiled=True),
-            preferred_element_type=jnp.float32,
-        )
-        * scale
-    )
+    product = jnp.dot(hidden, _serve_tracks(weight), preferred_element_type=jnp.float32) * scale
     partials = lax.optimization_barrier(product.astype(jnp.bfloat16)).astype(jnp.float32)
     return lax.psum_scatter(
         partials.astype(jnp.bfloat16), "tp", scatter_dimension=1, tiled=True

time: 787 us -> 777 us (0.987)
  waiting for transfers between devices: 627 us -> 597 us
  local copies, waits for them, and re-layouts: 3.01 us -> 21.9 us
    all_gather x2, waiting for transfers between devices: 214 us -> 134 us  [_serve_tracks(): frame_out = lax.all_gather(x_local, 'fs')]
    all_gather x1, waiting for transfers between devices: 1.79 us -> 43.2 us  [per_device(): lax.all_gather(mixer_low[1], 'fs', axis=0, tiled=True)]
    reshape x0 -> x2, local copies, waits for them, and re-layouts: none -> 19.3 us  [_serve_tracks(): return jnp.concatenate(frame_out, axis=1)]
    all_gather x1, waiting for transfers between devices: 149 us -> 161 us  [per_device(): lax.all_gather(channel_low[0], 'fs', axis=0, tiled=True)]
  transfers between devices with their start and end apart: 11 -> 11, of which waited for: 9 -> 8; matrix products, arithmetic and copies ran while one was open for 3% -> 7% of each run, Pallas kernels for 0% -> 0%
where the time goes in v1:
time: 777 us; the launch traced here: 776 us
  waiting for transfers between devices  597 us (77%)
  blocking collectives  83.5 us (11%)
  matrix products  40.2 us (5%)
  local copies, waits for them, and re-layouts  21.9 us (3%)
  other arithmetic  18.7 us (2%)
  between operations  14.7 us (2%)
    all_gather x1, waiting for transfers between devices, per_device(): lax.all_gather(channel_low[0], 'fs', axis=0, tiled=True)  161 us
    all_gather x1, waiting for transfers between devices, per_device(): lax.all_gather(channel_low[1], 'fs', axis=0, tiled=True)  153 us
    all_gather x2, waiting for transfers between devices, _serve_tracks(): frame_out = lax.all_gather(x_local, 'fs')  134 us
    all_gather x1, waiting for transfers between devices, per_device(): lax.all_gather(mixer_low[2], 'fs', axis=0, tiled=True)  46.7 us
    all_gather x1, waiting for transfers between devices, per_device(): lax.all_gather(mixer_low[0], 'fs', axis=0, tiled=True)  46.4 us
    all_gather x1, waiting for transfers between devices, per_device(): lax.all_gather(mixer_low[1], 'fs', axis=0, tiled=True)  43.2 us
    unnamed x1, blocking collectives  40 us
    dot_general x2, matrix products, project_back(): jnp.dot(hidden, _serve_tracks(weight), preferred_element_type=jnp.float32)  23.5 us
  transfers between devices with their start and end apart: 11, of which 8 were waited for; matrix products, arithmetic and copies ran while one was open for 7% of the time, Pallas kernels for 0%

profile of v1, /device:TPU:0, one launch (start us, length us, event | category | flops | bytes accessed | tf_op | source)
XLA Modules:
  0.0 776.2 jit_solution(6040730822287608760)
XLA Ops:
  6.5 1.9 convert_element_type.73
  8.4 0.0 all-gather.28.cloned.1.call-update
  8.5 0.0 all-gather.14.cloned.1.call-start
  8.5 1.4 fusion.4
  9.9 2.8 psum.14
  12.6 1.7 fusion.6
  14.4 0.0 copy-start.10
  14.4 0.0 copy-start.11
  14.4 0.0 all-gather.14.cloned.1.call-update
  14.5 0.0 all-gather.18.cloned.1.call-start
  14.5 0.7 convert_element_type.70
  15.3 0.0 all-gather.18.cloned.1.call-update
  15.3 0.0 all-gather.20.cloned.1.call-start
  15.3 0.7 convert_element_type.71
  16.1 0.0 all-gather.20.cloned.1.call-update
  16.1 0.0 all-gather.16.cloned.1.call-start
  16.2 0.7 convert_element_type.69
  16.9 0.0 all-gather.16.cloned.1.call-update
  16.9 0.0 reduce-scatter.3.cloned.1.call-start
  17.0 0.6 dynamic-slice
  18.9 0.2 dynamic-update-slice
  19.1 0.2 dynamic-update-slice.1
  19.3 0.2 dynamic-update-slice.2
  19.6 0.3 dynamic-update-slice.3
  19.8 0.3 dynamic-update-slice.4
  20.1 40.0 %all-reduce.7 = (f32[512]{0:T(512)S(1)}, f32[512]{0:T(512)S(1)}, f32[512]{0:T(512)}, f32[2816]{0:T(1024)}, f32[2816]{0:T(1024)}) all-reduce(f32[512]{0:T(512)S(1)} %dynamic-update-slice.1, f32[512]{0:T(512)S(1)} %dynamic-update-slice.2, f32[512]{0:T(512)S(1)} %dynamic-update-slice, ...), channel_id=1, replica_groups=mesh['rep'=2,'fs'=8,'tp'=2] {'fs'}, use_global_device_ids=true, to_apply=%add.3 | all-reduce | flops 7168 | bytes 57344
  60.1 16.3 %all-gather.2 = f32[8,1,256]{2,1,0:T(1,128)S(1)} all-gather(f32[1,1,256]{2,1,0:T(1,128)S(1)} %bitcast.64), channel_id=1, replica_groups=mesh['rep'=2,'fs'=8,'tp'=2] {'fs'}, dimensions={0}, use_global_device_ids=true | all-gather | bytes 9216 | tf_op jit(solution)/shard_map/all_gather | solution.py:79
  76.4 0.6 fusion.30
  76.9 3.9 copy.23
  80.9 43.2 %all-gather.18.cloned.1.call-done = bf16[2048,512]{1,0:T(8,128)(2,1)} async-done(((bf16[256,512]{1,0:T(8,128)(2,1)}), bf16[2048,512]{1,0:T(8,128)(2,1)}) %all-gather.18.cloned.1.call-update) | async-done | bytes 2097168 | tf_op jit(solution)/shard_map/all_gather | solution.py:93
  124.1 2.9 convolution_multiply_fusion.5
  127.0 46.7 %all-gather.20.cloned.1.call-done = bf16[2048,512]{1,0:T(8,128)(2,1)} async-done(((bf16[256,512]{1,0:T(8,128)(2,1)}), bf16[2048,512]{1,0:T(8,128)(2,1)}) %all-gather.20.cloned.1.call-update) | async-done | bytes 2097168 | tf_op jit(solution)/shard_map/all_gather | solution.py:94
  173.7 3.3 fusion.12
  177.0 46.4 %all-gather.16.cloned.1.call-done = bf16[2048,512]{1,0:T(8,128)(2,1)} async-done(((bf16[256,512]{1,0:T(8,128)(2,1)}), bf16[2048,512]{1,0:T(8,128)(2,1)}) %all-gather.16.cloned.1.call-update) | async-done | bytes 2097168 | tf_op jit(solution)/shard_map/all_gather | solution.py:92
  223.4 6.2 fusion.2
  229.5 0.0 reduce-scatter.3.cloned.1.call-update
  229.5 0.0 all-gather.30.cloned.1.call-start
  229.6 1.3 convert_element_type.82
  231.0 0.0 all-gather.30.cloned.1.call-update
  231.0 0.0 all-gather.22.cloned.1.call-start
  231.0 5.8 reduce-scatter.3.cloned.1.call-done
  236.9 1.4 fusion.8
  238.2 2.5 psum.15
  240.7 2.2 fusion.10
  242.9 0.0 all-gather.22.cloned.1.call-update
  242.9 0.0 all-gather.24.cloned.1.call-start
  243.0 1.3 convert_element_type.79
  244.2 0.0 all-gather.24.cloned.1.call-update
  244.3 0.0 copy-start.13
  244.3 0.0 all-gather.26.cloned.1.call-start
  244.3 3.1 convert_element_type.80
  247.4 0.0 all-gather.26.cloned.1.call-update
  247.4 0.0 reduce-scatter.5.cloned.1.call-start
  247.5 22.1 %all-gather.3 = f32[8,1,256]{2,1,0:T(1,128)S(1)} all-gather(f32[1,1,256]{2,1,0:T(1,128)S(1)} %bitcast.65), channel_id=1, replica_groups=mesh['rep'=2,'fs'=8,'tp'=2] {'fs'}, dimensions={0}, use_global_device_ids=true | all-gather | bytes 9216 | tf_op jit(solution)/shard_map/all_gather | solution.py:80
  269.6 0.1 slice_reduce_fusion.2
  269.7 133.9 %all-gather.30.cloned.1.call-done = bf16[22528,256]{1,0:T(8,128)(2,1)} async-done(((bf16[2816,256]{1,0:T(8,128)(2,1)}), bf16[22528,256]{1,0:T(8,128)(2,1)}) %all-gather.30.cloned.1.call-update) | async-done | bytes 11534352 | tf_op jit(solution)/shard_map/all_gather | solution.py:11
  403.6 15.3 %copy.24 = bf16[2816,8,256]{0,2,1:T(8,128)(2,1)} copy(bf16[2816,8,256]{2,0,1:T(8,128)(2,1)} %bitcast.55) | data formatting | bytes 23068672 | tf_op jit(solution)/shard_map/reshape | solution.py:12
  419.0 160.5 %all-gather.24.cloned.1.call-done = bf16[2048,2816]{1,0:T(8,128)(2,1)} async-done(((bf16[256,2816]{1,0:T(8,128)(2,1)}), bf16[2048,2816]{1,0:T(8,128)(2,1)}) %all-gather.24.cloned.1.call-update) | async-done | bytes 11534352 | tf_op jit(solution)/shard_map/all_gather | solution.py:106
  579.5 10.5 %convolution_multiply_fusion.1 = f32[320,2816]{1,0:T(8,128)} fusion(bf16[320,2048]{1,0:T(8,128)(2,1)} %all-gather.22.cloned.1.call-done, bf16[2048,2816]{1,0:T(8,128)(2,1)} %all-gather.24.cloned.1.call-done, f32[2816]{0:T(1024)S(1)} %copy-done.18), kind=kOutput, calls=%fused_computation.2 | convolution fusion | flops 3691888640 | bytes 16460800 | tf_op jit(solution)/shard_map/dot_general | solution.py:37
  590.0 153.0 %all-gather.26.cloned.1.call-done = bf16[2048,2816]{1,0:T(8,128)(2,1)} async-done(((bf16[256,2816]{1,0:T(8,128)(2,1)}), bf16[2048,2816]{1,0:T(8,128)(2,1)}) %all-gather.26.cloned.1.call-update) | async-done | bytes 11534352 | tf_op jit(solution)/shard_map/all_gather | solution.py:107
  743.1 17.4 %fusion.3 = bf16[320,2048]{1,0:T(8,128)(2,1)} fusion(bf16[2816,2048]{0,1:T(8,128)(2,1)} %bitcast.56, f32[2048]{0:T(1024)S(1)} %bitcast.60, bf16[320,2048]{1,0:T(8,128)(2,1)S(1)} %copy-done.15, bf16[2048,2816]{1,0:T(8,128)(2,1)} %all-gather.26.cloned.1.call-done, f32[320,2816]{1,0:T(8,128)} %convolution_multiply_fusion.1, f32[1,320,2816]{2,1,0:T(8,128)} %bitcast.66, ...), kind=kOutput, calls=%fused_computation.9 | convolution fusion | flops 7395000320 | bytes 32963584 | tf_op jit(solution)/shard_map/dot_general | solution.py:44
  760.5 0.0 reduce-scatter.5.cloned.1.call-update
  760.5 7.0 reduce-scatter.5.cloned.1.call-done
  767.5 2.3 fusion.11
  (54 shorter events, 0.1 us)
Async XLA Ops:
  6.5 6.1 copy-start
  6.5 8.0 %copy-start.4 = (f32[256,512]{1,0:T(8,128)S(1)}, f32[256,512]{1,0:T(8,128)}, u32[]{:S(2)}) copy-start(f32[256,512]{1,0:T(8,128)} %param.23) | copy-start | bytes 1572868
  6.5 70.4 %all-gather.28.cloned.1.call-start = ((), (), s32[]{:S(2)}) async-start(), calls=%async_computation.11 | async-start | bytes 2359296 | tf_op jit(solution)/shard_map/all_gather | solution.py:11
  8.4 6.9 copy-start.5
  8.5 72.4 %all-gather.14.cloned.1.call-start = ((), (), s32[]{:S(2)}) async-start(), calls=%async_computation.2 | async-start | bytes 1966080 | tf_op jit(solution)/shard_map/all_gather | solution.py:21
  9.9 6.3 copy-start.6
  14.4 2.6 copy-start.22
  14.4 4.5 copy-start.19
  14.4 4.7 copy-start.20
  14.4 5.0 copy-start.21
  14.4 5.2 copy-start.10
  14.4 5.4 copy-start.11
  14.4 45.7 %copy-start.12 = (f32[256]{0:T(256)S(1)}, f32[256]{0:T(256)}, u32[]{:S(2)}) copy-start(f32[256]{0:T(256)} %param.30) | copy-start | bytes 3076
  14.4 61.9 %copy-start.8 = (f32[3,512]{1,0:T(4,128)S(1)}, f32[3,512]{1,0:T(4,128)}, u32[]{:S(2)}) copy-start(f32[3,512]{1,0:T(4,128)} %param.28) | copy-start | bytes 18436
  14.5 109.6 %all-gather.18.cloned.1.call-start = ((), (), s32[]{:S(2)}) async-start(), calls=%async_computation.4 | async-start | bytes 2359296 | tf_op jit(solution)/shard_map/all_gather | solution.py:93
  15.3 158.5 %all-gather.20.cloned.1.call-start = ((), (), s32[]{:S(2)}) async-start(), calls=%async_computation.5 | async-start | bytes 2359296 | tf_op jit(solution)/shard_map/all_gather | solution.py:94
  16.1 207.3 %all-gather.16.cloned.1.call-start = ((), (), s32[]{:S(2)}) async-start(), calls=%async_computation.3 | async-start | bytes 2359296 | tf_op jit(solution)/shard_map/all_gather | solution.py:92
  16.9 219.9 %reduce-scatter.3.cloned.1.call-start = ((), (), s32[]{:S(2)}) async-start(), calls=%async_computation.6 | async-start | bytes 1966080 | tf_op jit(solution)/shard_map/reduce_scatter | solution.py:46
  124.1 49.6 %copy-start.14 = (bf16[320,2048]{1,0:T(8,128)(2,1)S(1)}, bf16[320,2048]{1,0:T(8,128)(2,1)}, u32[]{:S(2)}) copy-start(bf16[320,2048]{1,0:T(8,128)(2,1)} %all-gather.14.cloned.1.call-done) | copy-start | bytes 3932164
  223.4 6.2 copy-start.2
  229.5 174.1 %all-gather.30.cloned.1.call-start = ((), (), s32[]{:S(2)}) async-start(), calls=%async_computation.12 | async-start | bytes 12976128 | tf_op jit(solution)/shard_map/all_gather | solution.py:11
  230.9 9.8 %copy-start.9 = (f32[1024]{0:T(1024)S(1)}, f32[1024]{0:T(1024)}, u32[]{:S(2)}) copy-start(f32[1024]{0:T(1024)} %param.31) | copy-start | bytes 12292
  231.0 12.0 %copy-start.3 = (f32[256,2816]{1,0:T(8,128)S(1)}, f32[256,2816]{1,0:T(8,128)}, u32[]{:S(2)}) copy-start(f32[256,2816]{1,0:T(8,128)} %param.32) | copy-start | bytes 8650756
  231.0 188.0 %all-gather.22.cloned.1.call-start = ((), (), s32[]{:S(2)}) async-start(), calls=%async_computation.7 | async-start | bytes 1966080 | tf_op jit(solution)/shard_map/all_gather | solution.py:21
  242.9 336.6 %all-gather.24.cloned.1.call-start = ((), (), s32[]{:S(2)}) async-start(), calls=%async_computation.8 | async-start | bytes 12976128 | tf_op jit(solution)/shard_map/all_gather | solution.py:106
  244.3 3.2 copy-start.13
  244.3 25.3 %copy-start.7 = (f32[3,2816]{1,0:T(4,128)S(1)}, f32[3,2816]{1,0:T(4,128)}, u32[]{:S(2)}) copy-start(f32[3,2816]{1,0:T(4,128)} %param.36) | copy-start | bytes 101380
  244.3 498.8 %all-gather.26.cloned.1.call-start = ((), (), s32[]{:S(2)}) async-start(), calls=%async_computation.9 | async-start | bytes 12976128 | tf_op jit(solution)/shard_map/all_gather | solution.py:107
  247.4 520.0 %reduce-scatter.5.cloned.1.call-start = ((), (), s32[]{:S(2)}) async-start(), calls=%async_computation.10 | async-start | bytes 1966080 | tf_op jit(solution)/shard_map/reduce_scatter | solution.py:46
  403.6 175.9 %copy-start.18 = (f32[2816]{0:T(1024)S(1)}, f32[2816]{0:T(1024)}, u32[]{:S(2)}) copy-start(f32[2816]{0:T(1024)} %get-tuple-element.11) | copy-start | bytes 33796
  579.5 163.6 %copy-start.15 = (bf16[320,2048]{1,0:T(8,128)(2,1)S(1)}, bf16[320,2048]{1,0:T(8,128)(2,1)}, u32[]{:S(2)}) copy-start(bf16[320,2048]{1,0:T(8,128)(2,1)} %all-gather.22.cloned.1.call-done) | copy-start | bytes 3932164
  579.5 163.6 %copy-start.16 = (f32[2816]{0:T(1024)S(1)}, f32[2816]{0:T(1024)}, u32[]{:S(2)}) copy-start(f32[2816]{0:T(1024)} %param.37) | copy-start | bytes 33796
  579.5 163.6 %copy-start.17 = (f32[2816]{0:T(1024)S(1)}, f32[2816]{0:T(1024)}, u32[]{:S(2)}) copy-start(f32[2816]{0:T(1024)} %get-tuple-element.12) | copy-start | bytes 33796
  743.1 24.4 %copy-start.1 = (bf16[320,1024]{1,0:T(8,128)(2,1)S(1)}, bf16[320,1024]{1,0:T(8,128)(2,1)}, u32[]{:S(2)}) copy-start(bf16[320,1024]{1,0:T(8,128)(2,1)} %reduce-scatter.3.cloned.1.call-done) | copy-start | bytes 1966084
Sparse Core Ops, SparseCore 0:
  9.5 52.4 all-gather.27
  63.5 8.0 all-gather.13
  73.8 50.2 all-gather.17
  126.1 47.6 all-gather.19
  175.7 47.6 all-gather.15
  229.7 7.1 reduce-scatter.2
  239.0 164.5 all-gather.29
  405.2 7.5 all-gather.21
  415.0 164.4 all-gather.23
  581.5 161.4 all-gather.25
  760.6 6.8 reduce-scatter.4
